TPU v7x, 32 devices: a whole 2x2x4 slice. The times are simulated.
32 devices in a mesh: fs: 8 (over z, x), tp: 4 (over y, core).
Axes of the slice: x: 2, y: 2, z: 4, core: 2. Of those that a mesh axis runs over, the one named last changes fastest.
Arguments:
- saved_input: bfloat16 [24576, 2048], P('fs'), may hold values from -6 to 6
- proj_cot: bfloat16 [3, 24576, 2048], P(None, 'fs', 'tp'), may hold values from -0.0390625 to 0.0390625
- log_cache: float32 [16, 24576], P(None, 'fs'), as said below
- cache_cot: float32 [16, 24576], P(None, 'fs'), may hold values from -0.0390625 to 0.0390625
- proj_master: float32 [3, 2048, 2048], P(None, 'fs', 'tp'), may hold values from -0.125 to 0.125
- factors: bfloat16 [3, 2048, 256], P(None, 'fs'), may hold values from -0.125 to 0.125
- first_moment: float32 [3, 256, 2048], P(None, None, 'tp'), may hold values from -6 to 6
- second_moment: float32 [3, 256, 2048], P(None, None, 'tp'), may hold values from 0.01 to 10
- gate_master: float32 [16, 2048], replicated, may hold values from -0.125 to 0.125
- gate_first: float32 [16, 2048], replicated, may hold values from -6 to 6
- gate_second: float32 [16, 2048], replicated, may hold values from 0.1 to 3
Outputs:
- proj_step: float32 [3, 2048, 2048], P(None, 'fs', 'tp')
- proj_new: float32 [3, 2048, 2048], P(None, 'fs', 'tp')
- proj_copy: bfloat16 [3, 2048, 2048], P(None, None, 'tp')
- first_new: float32 [3, 256, 2048], P(None, None, 'tp')
- second_new: float32 [3, 256, 2048], P(None, None, 'tp')
- gate_new: float32 [16, 2048], replicated
- gate_copy: bfloat16 [16, 2048], replicated
- gate_first_new: float32 [16, 2048], replicated
- gate_second_new: float32 [16, 2048], replicated
Inputs may be any that keep to these rules, and one draw needn't show every extreme that they name: `log_cache`: each head's values never rise along positions.
All inputs are finite; a program needn't handle non-finite values.
Results may differ from a plain program's by a relative error of at most 0.0004.
Values may be sent and summed in bfloat16 or wider, within the bound.
A program may use at most 128 MiB of HBM per device.

v0:
```python
import jax
import jax.numpy as jnp
from jax import lax
from jax.sharding import PartitionSpec as P

BETA_ONE = 0.8
BETA_TWO = 0.9
LEARN = 0.001


def from_behind(x, axis, by):
    peers = lax.axis_size(axis)
    pairs = [(i, i + by) for i in range(peers) if 0 <= i + by < peers]
    return lax.ppermute(x, axis, pairs)


def prefix(value, axis, join, neutral):
    count, mine = (lax.axis_size(axis), lax.axis_index(axis))
    pieces = lax.all_gather(value, axis)
    pieces = pieces[::-1]
    mine = count - 1 - mine
    so_far = jnp.full_like(value, 0) + jnp.asarray(neutral, value.dtype)

    def hop(position, so_far):
        longer = join(so_far, pieces[position])
        return jnp.where(position < mine, longer, so_far)

    return lax.fori_loop(0, count - 1, hop, so_far)


def add_pair(earlier, later_part):
    return earlier + later_part


def local(
    saved_input,
    proj_cot,
    log_cache,
    cache_cot,
    proj_master,
    factors,
    first_moment,
    second_moment,
    gate_master,
    gate_first,
    gate_second,
):
    heads = log_cache.shape[0]
    edge = from_behind(log_cache[:, -1:], "fs", 1)
    previous = jnp.concatenate([edge, log_cache[:, :-1]], axis=1)
    gate_logarithm = log_cache - previous
    carried = prefix(jnp.sum(cache_cot, axis=1), "fs", add_pair, jnp.zeros((heads,), jnp.float32))
    later = jnp.flip(jnp.cumsum(jnp.flip(cache_cot, 1), axis=1), 1) + carried[:, None]
    gate_cot = (later * -jnp.expm1(gate_logarithm)).astype(jnp.bfloat16)
    gate_part = jnp.dot(gate_cot, saved_input, preferred_element_type=jnp.float32)
    all_factors = lax.all_gather(factors, "fs", axis=1, tiled=True)
    reduced = jnp.einsum(
        "td,rdk->rtk", saved_input, all_factors, preferred_element_type=jnp.float32
    )
    upper_half = lax.optimization_barrier(reduced.astype(jnp.bfloat16))
    lower_half = (reduced - upper_half.astype(jnp.float32)).astype(jnp.bfloat16)
    low_part = jnp.einsum("rtk,rtw->rkw", upper_half, proj_cot, preferred_element_type=jnp.float32)
    low_part = low_part + jnp.einsum(
        "rtk,rtw->rkw", lower_half, proj_cot, preferred_element_type=jnp.float32
    )
    low, gate_grad = lax.psum((low_part, gate_part), "fs")
    first_new = BETA_ONE * first_moment + (1.0 - BETA_ONE) * low
    second_new = BETA_TWO * second_moment + (1.0 - BETA_TWO) * low * low
    direction = first_new / jnp.sqrt(second_new)
    squares = lax.psum(jnp.sum(direction * direction), "tp")
    entries = direction.shape[0] * direction.shape[1] * direction.shape[2] * lax.axis_size("tp")
    scale = lax.rsqrt(squares / entries + 1e-06)
    product = jnp.einsum(
        "rdk,rkw->rdw", factors.astype(jnp.float32), direction, precision=lax.Precision.HIGHEST
    )
    proj_step = scale * product
    proj_new = proj_master - LEARN * proj_step
    proj_copy = lax.all_gather(proj_new.astype(jnp.bfloat16), "fs", axis=1, tiled=True)
    gate_first_new = BETA_ONE * gate_first + (1.0 - BETA_ONE) * gate_grad
    gate_second_new = BETA_TWO * gate_second + (1.0 - BETA_TWO) * gate_grad * gate_grad
    gate_new = gate_master - LEARN * gate_first_new / jnp.sqrt(gate_second_new)
    gate_copy = gate_new.astype(jnp.bfloat16)
    return (
        proj_step,
        proj_new,
        proj_copy,
        first_new,
        second_new,
        gate_new,
        gate_copy,
        gate_first_new,
        gate_second_new,
    )


def solution(mesh):
    placed = (
        P("fs", None),
        P(None, "fs", "tp"),
        P(None, "fs"),
        P(None, "fs"),
        P(None, "fs", "tp"),
        P(None, "fs", None),
        P(None, None, "tp"),
        P(None, None, "tp"),
        P(),
        P(),
        P(),
    )
    return jax.shard_map(
        local,
        mesh=mesh,
        in_specs=placed,
        out_specs=(
            P(None, "fs", "tp"),
            P(None, "fs", "tp"),
            P(None, None, "tp"),
            P(None, None, "tp"),
            P(None, None, "tp"),
            P(),
            P(),
            P(),
            P(),
        ),
        check_vma=False,
    )
```

profile of v0, /device:TPU:0, one launch (start us, length us, event | category | flops | bytes accessed | tf_op | source)
XLA Modules:
  0.0 330.7 jit_solution(11614293912108282255)
XLA Ops:
  7.2 2.0 copy.26
  9.3 0.8 slice.14
  10.1 4.9 %collective-permute-start = (f32[16,1]{1,0:T(8,128)S(1)}, f32[16,1]{1,0:T(8,128)S(1)}, u32[]{:S(2)}, u32[]{:S(2)}) collective-permute-start(f32[16,1]{1,0:T(8,128)S(1)} %slice.14), channel_id=1, source_target_pairs={{0,4},{4,8},{8,12},{12,16},{16,20},{20,24},{24,28},{1,5},{5,9},{9,... | collective-permute-start | bytes 200 | tf_op jit(solution)/shard_map/ppermute | solution.py:14
  15.0 9.3 %rev.10 = f32[16,3072]{1,0:T(8,128)S(1)} reverse(f32[16,3072]{1,0:T(8,128)} %param.16), dimensions={1} | reverse | bytes 393216 | tf_op jit(solution)/shard_map/jit(_flip)/rev | solution.py:53
  24.5 4.6 %reduce-window.6 = f32[16,24,128]{2,1,0:T(8,128)S(1)} reduce-window(f32[16,24,128]{2,1,0:T(8,128)S(1)} %bitcast.36, f32[]{:T(128)} %constant.50.clone.1), window={size=1x1x128 pad=0_0x0_0x127_0}, to_apply=%region_3.4 | reduce-window | flops 6242304 | bytes 393220 | tf_op jit(solution)/shard_map/reduce-window
  29.7 0.6 dynamic-slice
  31.2 19.9 %all-reduce = f32[128]{0:T(128)S(1)} all-reduce(f32[128]{0:T(128)S(1)} %dynamic-update-slice), channel_id=2, replica_groups=mesh['fs'=8,'tp'=4] {'fs'}, use_global_device_ids=true, to_apply=%add | all-reduce | flops 128 | bytes 1024
  51.4 1.7 rev.11
  53.2 7.1 %fusion.14 = f32[16,2048]{1,0:T(8,128)} fusion(bf16[3072,2048]{1,0:T(8,128)(2,1)} %param.13, f32[16,3072]{1,0:T(8,128)S(1)} %copy-done.2, f32[16,3071]{1,0:T(8,128)S(1)} %bitcast.34, f32[16,1]{1,0:T(8,128)S(1)} %collective-permute-done, f32[16,3072]{1,0:T(8,128)S(1)} %rev.11, f32[16]{0:T(128)S(1)} %get-tuple-element.88), kind=kOutput, calls=%fused_computation.27 | convolution fusion | flops 201621504 | bytes 13303872 | tf_op jit(solution)/shard_map/dot_general | solution.py:55
  60.3 15.9 %all-gather.4.cloned.1.call-done = bf16[3,2048,256]{1,2,0:T(8,128)(2,1)} async-done(((bf16[3,256,256]{1,2,0:T(8,128)(2,1)}), bf16[3,2048,256]{1,2,0:T(8,128)(2,1)}) %all-gather.4.cloned.1.call-update) | async-done | bytes 3145744 | tf_op jit(solution)/shard_map/all_gather | solution.py:56
  76.1 16.1 %bitcast_convert_fusion = (bf16[3,3072,256]{1,2,0:T(8,128)(2,1)S(1)}, f32[3,256,3072]{2,1,0:T(8,128)}) fusion(bf16[3,2048,256]{1,2,0:T(8,128)(2,1)} %all-gather.4.cloned.1.call-done, bf16[3072,2048]{1,0:T(8,128)(2,1)} %param.13), kind=kOutput, calls=%fused_computation.5 | convolution fusion | flops 9666035712 | bytes 29884416 | tf_op jit(solution)/shard_map/td,rdk->rtk/dot_general | solution.py:57
  92.2 5.3 %fusion.22 = f32[3,256,512]{2,1,0:T(8,128)S(1)} fusion(bf16[3,3072,256]{1,2,0:T(8,128)(2,1)S(1)} %get-tuple-element.141, bf16[3,3072,512]{2,1,0:T(8,128)(2,1)} %param.14), kind=kOutput, calls=%fused_computation.33 | convolution fusion | flops 2415919104 | bytes 15728640 | tf_op jit(solution)/shard_map/rtk,rtw->rkw/dot_general | solution.py:62
  97.6 10.2 %fusion.6 = f32[3,256,512]{2,1,0:T(8,128)} fusion(f32[3,256,512]{2,1,0:T(8,128)S(1)} %fusion.22, bf16[3,3072,512]{2,1,0:T(8,128)(2,1)} %param.14, f32[3,256,3072]{2,1,0:T(8,128)} %get-tuple-element.142, bf16[3,3072,256]{1,2,0:T(8,128)(2,1)S(1)} %get-tuple-element.141), kind=kOutput, calls=%fused_computation.15 | convolution fusion | flops 2423390208 | bytes 26738688 | tf_op jit(solution)/shard_map/rtk,rtw->rkw/dot_general | solution.py:63
  107.9 1.3 copy-done.1
  109.2 0.5 copy.28
  109.7 89.2 %all-reduce.4.cloned.1.call-done = (f32[3,256,512]{2,1,0:T(8,128)}, f32[16,2048]{1,0:T(8,128)}) async-done(((f32[3,256,512]{2,1,0:T(8,128)}, f32[16,2048]{1,0:T(8,128)}), (f32[3,256,512]{2,1,0:T(8,128)}, f32[16,2048]{1,0:T(8,128)})) %all-reduce.4.cloned.1.call-update) | async-done | bytes 1703952 | tf_op jit(solution)/shard_map/psum | solution.py:66
  198.9 5.5 %multiply_reduce_fusion = (f32[]{:T(128)}, f32[3,256,512]{2,1,0:T(8,128)}, f32[3,256,512]{2,1,0:T(8,128)}) fusion(f32[3,256,512]{2,1,0:T(8,128)} %get-tuple-element.130, f32[3,256,512]{2,1,0:T(8,128)} %param.20, f32[3,256,512]{2,1,0:T(8,128)} %param.19), kind=kLoop, calls=%fused_computation.12 | loop fusion | flops 3932159 | bytes 7864324 | tf_op jit(solution)/shard_map/reduce_sum | solution.py:70
  204.4 7.6 %psum.22 = f32[]{:T(128)} all-reduce(f32[]{:T(128)} %get-tuple-element.138), channel_id=1, replica_groups=mesh['fs'=8,'tp'=4] {'tp'}, use_global_device_ids=true, to_apply=%region_2.3 | all-reduce | flops 1 | bytes 8 | tf_op jit(solution)/shard_map/psum | solution.py:70
  212.7 4.8 %fusion.20 = (bf16[3,256,512]{1,2,0:T(8,128)(2,1)}, f32[3,256,512]{1,2,0:T(8,128)S(1)}, f32[3,256,512]{1,2,0:T(8,128)}) fusion(f32[3,256,512]{1,2,0:T(8,128)S(1)} %copy.28, bf16[3,256,256]{2,1,0:T(8,128)(2,1)S(1)} %copy-done, f32[3,256,512]{2,1,0:T(8,128)} %get-tuple-element.140, f32[3,256,512]{2,1,0:T(8,128)} %get-tuple-element.139, f32[]{:T(128)S(6)} %rsqrt.5), kind=kOutput, calls=%fused_computation.32 | convolution fusion | flops 1209925632 | bytes 9043972 | tf_op jit(solution)/shard_map/rdk,rkw->rdw/dot_general | solution.py:73
  217.5 3.0 copy.29
  220.6 1.6 copy.30
  222.2 0.8 fusion.18
  223.0 92.6 %all-gather.6.cloned.1.call-done = bf16[3,2048,512]{1,2,0:T(8,128)(2,1)} async-done(((bf16[3,256,512]{1,2,0:T(8,128)(2,1)}), bf16[3,2048,512]{1,2,0:T(8,128)(2,1)}) %all-gather.6.cloned.1.call-update) | async-done | bytes 6291472 | tf_op jit(solution)/shard_map/all_gather | solution.py:78
  315.6 8.6 %copy.31 = bf16[3,2048,512]{2,1,0:T(8,128)(2,1)} copy(bf16[3,2048,512]{1,2,0:T(8,128)(2,1)} %all-gather.6.cloned.1.call-done) | data formatting | bytes 12582912
  (43 shorter events, 1.7 us)
Async XLA Ops:
  7.2 17.2 %copy-start.3 = (f32[16,3072]{1,0:T(8,128)S(1)}, f32[16,3072]{1,0:T(8,128)}, u32[]{:S(2)}) copy-start(f32[16,3072]{1,0:T(8,128)} %param.16) | copy-start | bytes 589828
  7.2 68.9 %all-gather.4.cloned.1.call-start = ((), (), s32[]{:S(2)}) async-start(), calls=%async_computation | async-start | bytes 3538944 | tf_op jit(solution)/shard_map/all_gather | solution.py:56
  9.2 20.5 %copy-start.8 = (u32[32]{0:T(128)S(1)}, u32[32]{0:T(128)}, u32[]{:S(2)}) copy-start(u32[32]{0:T(128)} %constant.60) | copy-start | bytes 388
  9.2 43.9 %copy-start.2 = (f32[16,3072]{1,0:T(8,128)S(1)}, f32[16,3072]{1,0:T(8,128)}, u32[]{:S(2)}) copy-start(f32[16,3072]{1,0:T(8,128)} %param.15) | copy-start | bytes 589828
  9.2 189.7 %all-reduce.4.cloned.1.call-start = ((), (), s32[]{:S(2)}) async-start(), calls=%async_computation.2 | async-start | bytes 3407872 | tf_op jit(solution)/shard_map/psum | solution.py:66
  10.1 43.1 %collective-permute-start = (f32[16,1]{1,0:T(8,128)S(1)}, f32[16,1]{1,0:T(8,128)S(1)}, u32[]{:S(2)}, u32[]{:S(2)}) collective-permute-start(f32[16,1]{1,0:T(8,128)S(1)} %slice.14), channel_id=1, source_target_pairs={{0,4},{4,8},{8,12},{12,16},{16,20},{20,24},{24,28},{1,5},{5,9},{9,... | collective-permute-start | bytes 200 | tf_op jit(solution)/shard_map/ppermute | solution.py:14
  107.8 1.4 copy-start.1
  107.8 207.7 %all-gather.6.cloned.1.call-start = ((), (), s32[]{:S(2)}) async-start(), calls=%async_computation.1 | async-start | bytes 7077888 | tf_op jit(solution)/shard_map/all_gather | solution.py:78
  198.9 13.8 %copy-start = (bf16[3,256,256]{2,1,0:T(8,128)(2,1)S(1)}, bf16[3,256,256]{2,1,0:T(8,128)(2,1)}, u32[]{:S(2)}) copy-start(bf16[3,256,256]{2,1,0:T(8,128)(2,1)} %param.18) | copy-start | bytes 1179652
  220.6 1.6 copy-start.4
  220.6 1.6 copy-start.5
  220.6 1.6 copy-start.6
  220.6 1.6 copy-start.7
Sparse Core Ops, SparseCore 0:
  10.6 65.4 all-gather.3
  107.9 90.9 all-reduce.3
  217.7 97.8 all-gather.5
where the time goes:
time: 332 us; the launch traced here: 331 us
  waiting for transfers between devices  198 us (60%)
  matrix products  43.6 us (13%)
  local copies, waits for them, and re-layouts  30.1 us (9%)
  blocking collectives  27.5 us (8%)
  between operations  15.3 us (5%)
  other arithmetic  11.4 us (3%)
  starting transfers between devices  4.98 us (2%)
    all_gather x1, waiting for transfers between devices, local(): lax.all_gather(proj_new.astype(jnp.bfloat16), 'fs', axis=1, tiled=True)  92.6 us
    psum x1, waiting for transfers between devices, local(): low, gate_grad = lax.psum((low_part, gate_part), 'fs')  89.2 us
    unnamed x1, blocking collectives  19.9 us
    unnamed x28, local copies, waits for them, and re-layouts  17.9 us
    dot_general x1, matrix products, local(): jnp.einsum('td,rdk->rtk', saved_input, all_factors, preferred_element_typ...  16.1 us
    all_gather x1, waiting for transfers between devices, local(): all_factors = lax.all_gather(factors, 'fs', axis=1, tiled=True)  15.9 us
    dot_general x1, matrix products, local(): jnp.einsum('rtk,rtw->rkw', lower_half, proj_cot, preferred_element_type=j...  10.2 us
    rev x1, local copies, waits for them, and re-layouts, local(): jnp.flip(cache_cot, 1)  9.35 us
  transfers between devices with their start and end apart: 4, of which 3 were waited for; matrix products, arithmetic and copies ran while one was open for 9% of the time, Pallas kernels for 0%

commit v1 on v0

--- a/solution.py
+++ b/solution.py
@@ -75,7 +75,9 @@
     )
     proj_step = scale * product
     proj_new = proj_master - LEARN * proj_step
-    proj_copy = lax.all_gather(proj_new.astype(jnp.bfloat16), "fs", axis=1, tiled=True)
+    block = proj_new.astype(jnp.bfloat16)
+    sent = jnp.stack([block] * lax.axis_size("fs"))
+    proj_copy = jnp.concatenate(lax.all_to_all(sent, "fs", 0, 0), axis=1)
     gate_first_new = BETA_ONE * gate_first + (1.0 - BETA_ONE) * gate_grad
     gate_second_new = BETA_TWO * gate_second + (1.0 - BETA_TWO) * gate_grad * gate_grad
     gate_new = gate_master - LEARN * gate_first_new / jnp.sqrt(gate_second_new)

time: 332 us -> 378 us (1.14)
  waiting for transfers between devices: 198 us -> 238 us
  starting transfers between devices: 4.98 us -> 9.83 us
    all_to_all x0 -> x1, waiting for transfers between devices: none -> 133 us  [local(): proj_copy = jnp.concatenate(lax.all_to_all(sent, 'fs', 0, 0), axis=1)]
    all_gather x1 -> x0, waiting for transfers between devices: 92.6 us -> none  [local(): lax.all_gather(proj_new.astype(jnp.bfloat16), 'fs', axis=1, tiled=True)]
    unnamed x28 -> x29, local copies, waits for them, and re-layouts: 17.9 us -> 7.97 us
    all_to_all x0 -> x1, local copies, waits for them, and re-layouts: none -> 6.09 us  [local(): proj_copy = jnp.concatenate(lax.all_to_all(sent, 'fs', 0, 0), axis=1)]
    all_to_all x0 -> x1, starting transfers between devices: none -> 4.89 us  [local(): proj_copy = jnp.concatenate(lax.all_to_all(sent, 'fs', 0, 0), axis=1)]
  transfers between devices with their start and end apart: 4 -> 4, of which waited for: 3 -> 3; matrix products, arithmetic and copies ran while one was open for 9% -> 8% of each run, Pallas kernels for 0% -> 0%
where the time goes in v1:
time: 378 us; the launch traced here: 377 us
  waiting for transfers between devices  238 us (63%)
  matrix products  43.6 us (12%)
  local copies, waits for them, and re-layouts  31.1 us (8%)
  blocking collectives  27.5 us (7%)
  between operations  15.6 us (4%)
  other arithmetic  11.4 us (3%)
  starting transfers between devices  9.83 us (3%)
    all_to_all x1, waiting for transfers between devices, local(): proj_copy = jnp.concatenate(lax.all_to_all(sent, 'fs', 0, 0), axis=1)  133 us
    psum x1, waiting for transfers between devices, local(): low, gate_grad = lax.psum((low_part, gate_part), 'fs')  89.2 us
    unnamed x1, blocking collectives  19.9 us
    dot_general x1, matrix products, local(): jnp.einsum('td,rdk->rtk', saved_input, all_factors, preferred_element_typ...  16.1 us
    all_gather x1, waiting for transfers between devices, local(): all_factors = lax.all_gather(factors, 'fs', axis=1, tiled=True)  15.9 us
    dot_general x1, matrix products, local(): jnp.einsum('rtk,rtw->rkw', lower_half, proj_cot, preferred_element_type=j...  10.2 us
    rev x1, local copies, waits for them, and re-layouts, local(): jnp.flip(cache_cot, 1)  9.35 us
    unnamed x29, local copies, waits for them, and re-layouts  7.97 us
  transfers between devices with their start and end apart: 4, of which 3 were waited for; matrix products, arithmetic and copies ran while one was open for 8% of the time, Pallas kernels for 0%

profile of v1, /device:TPU:0, one launch (start us, length us, event | category | flops | bytes accessed | tf_op | source)
XLA Modules:
  0.0 377.4 jit_solution(8041268441333437275)
XLA Ops:
  7.2 2.0 copy.38
  9.3 0.8 slice.14
  10.1 4.9 %collective-permute-start = (f32[16,1]{1,0:T(8,128)S(1)}, f32[16,1]{1,0:T(8,128)S(1)}, u32[]{:S(2)}, u32[]{:S(2)}) collective-permute-start(f32[16,1]{1,0:T(8,128)S(1)} %slice.14), channel_id=1, source_target_pairs={{0,4},{4,8},{8,12},{12,16},{16,20},{20,24},{24,28},{1,5},{5,9},{9,... | collective-permute-start | bytes 200 | tf_op jit(solution)/shard_map/ppermute | solution.py:14
  15.0 9.3 %rev.10 = f32[16,3072]{1,0:T(8,128)S(1)} reverse(f32[16,3072]{1,0:T(8,128)} %param.16), dimensions={1} | reverse | bytes 393216 | tf_op jit(solution)/shard_map/jit(_flip)/rev | solution.py:53
  24.5 4.6 %reduce-window.6 = f32[16,24,128]{2,1,0:T(8,128)S(1)} reduce-window(f32[16,24,128]{2,1,0:T(8,128)S(1)} %bitcast.40, f32[]{:T(128)} %constant.50.clone.1), window={size=1x1x128 pad=0_0x0_0x127_0}, to_apply=%region_3.4 | reduce-window | flops 6242304 | bytes 393220 | tf_op jit(solution)/shard_map/reduce-window
  31.2 19.9 %all-reduce = f32[128]{0:T(128)S(1)} all-reduce(f32[128]{0:T(128)S(1)} %dynamic-update-slice), channel_id=2, replica_groups=mesh['fs'=8,'tp'=4] {'fs'}, use_global_device_ids=true, to_apply=%add | all-reduce | flops 128 | bytes 1024
  51.4 1.7 rev.11
  53.2 7.1 %fusion.14 = f32[16,2048]{1,0:T(8,128)} fusion(bf16[3072,2048]{1,0:T(8,128)(2,1)} %param.13, f32[16,3072]{1,0:T(8,128)S(1)} %copy-done.3, f32[16,3071]{1,0:T(8,128)S(1)} %bitcast.38, f32[16,1]{1,0:T(8,128)S(1)} %collective-permute-done, f32[16,3072]{1,0:T(8,128)S(1)} %rev.11, f32[16]{0:T(128)S(1)} %get-tuple-element.88), kind=kOutput, calls=%fused_computation.27 | convolution fusion | flops 201621504 | bytes 13303872 | tf_op jit(solution)/shard_map/dot_general | solution.py:55
  60.3 15.9 %all-gather.3.cloned.1.call-done = bf16[3,2048,256]{1,2,0:T(8,128)(2,1)} async-done(((bf16[3,256,256]{1,2,0:T(8,128)(2,1)}), bf16[3,2048,256]{1,2,0:T(8,128)(2,1)}) %all-gather.3.cloned.1.call-update) | async-done | bytes 3145744 | tf_op jit(solution)/shard_map/all_gather | solution.py:56
  76.1 16.1 %bitcast_convert_fusion = (bf16[3,3072,256]{1,2,0:T(8,128)(2,1)S(1)}, f32[3,256,3072]{2,1,0:T(8,128)}) fusion(bf16[3,2048,256]{1,2,0:T(8,128)(2,1)} %all-gather.3.cloned.1.call-done, bf16[3072,2048]{1,0:T(8,128)(2,1)} %param.13), kind=kOutput, calls=%fused_computation.5 | convolution fusion | flops 9666035712 | bytes 29884416 | tf_op jit(solution)/shard_map/td,rdk->rtk/dot_general | solution.py:57
  92.2 5.3 %fusion.22 = f32[3,256,512]{2,1,0:T(8,128)S(1)} fusion(bf16[3,3072,256]{1,2,0:T(8,128)(2,1)S(1)} %get-tuple-element.159, bf16[3,3072,512]{2,1,0:T(8,128)(2,1)} %param.14), kind=kOutput, calls=%fused_computation.33 | convolution fusion | flops 2415919104 | bytes 15728640 | tf_op jit(solution)/shard_map/rtk,rtw->rkw/dot_general | solution.py:62
  97.6 10.2 %fusion.6 = f32[3,256,512]{2,1,0:T(8,128)} fusion(f32[3,256,512]{2,1,0:T(8,128)S(1)} %fusion.22, bf16[3,3072,512]{2,1,0:T(8,128)(2,1)} %param.14, f32[3,256,3072]{2,1,0:T(8,128)} %get-tuple-element.160, bf16[3,3072,256]{1,2,0:T(8,128)(2,1)S(1)} %get-tuple-element.159), kind=kOutput, calls=%fused_computation.15 | convolution fusion | flops 2423390208 | bytes 26738688 | tf_op jit(solution)/shard_map/rtk,rtw->rkw/dot_general | solution.py:63
  107.8 1.4 copy-done.2
  109.7 89.2 %all-reduce.4.cloned.1.call-done = (f32[3,256,512]{2,1,0:T(8,128)}, f32[16,2048]{1,0:T(8,128)}) async-done(((f32[3,256,512]{2,1,0:T(8,128)}, f32[16,2048]{1,0:T(8,128)}), (f32[3,256,512]{2,1,0:T(8,128)}, f32[16,2048]{1,0:T(8,128)})) %all-reduce.4.cloned.1.call-update) | async-done | bytes 1703952 | tf_op jit(solution)/shard_map/psum | solution.py:66
  198.9 5.5 %multiply_reduce_fusion = (f32[]{:T(128)}, f32[3,256,512]{2,1,0:T(8,128)}, f32[3,256,512]{2,1,0:T(8,128)}) fusion(f32[3,256,512]{2,1,0:T(8,128)} %get-tuple-element.148, f32[3,256,512]{2,1,0:T(8,128)} %param.20, f32[3,256,512]{2,1,0:T(8,128)} %param.19), kind=kLoop, calls=%fused_computation.12 | loop fusion | flops 3932159 | bytes 7864324 | tf_op jit(solution)/shard_map/reduce_sum | solution.py:70
  204.4 7.6 %psum.22 = f32[]{:T(128)} all-reduce(f32[]{:T(128)} %get-tuple-element.156), channel_id=1, replica_groups=mesh['fs'=8,'tp'=4] {'tp'}, use_global_device_ids=true, to_apply=%region_2.3 | all-reduce | flops 1 | bytes 8 | tf_op jit(solution)/shard_map/psum | solution.py:70
  212.7 4.8 %fusion.20 = (bf16[3,256,512]{1,2,0:T(8,128)(2,1)}, f32[3,256,512]{1,2,0:T(8,128)S(1)}, f32[3,256,512]{1,2,0:T(8,128)}) fusion(f32[3,256,512]{1,2,0:T(8,128)S(1)} %copy.40, bf16[3,256,256]{2,1,0:T(8,128)(2,1)S(1)} %copy-done.1, f32[3,256,512]{2,1,0:T(8,128)} %get-tuple-element.158, f32[3,256,512]{2,1,0:T(8,128)} %get-tuple-element.157, f32[]{:T(128)S(6)} %rsqrt.5), kind=kOutput, calls=%fused_computation.32 | convolution fusion | flops 1209925632 | bytes 9043972 | tf_op jit(solution)/shard_map/rdk,rkw->rdw/dot_general | solution.py:73
  217.5 1.4 copy.41
  218.9 3.4 stack.2
  222.3 4.9 %all-to-all-start = ((bf16[8,3,256,512]{3,2,1,0:T(8,128)(2,1)}), bf16[8,3,256,512]{3,2,1,0:T(8,128)(2,1)}, u32[]{:S(2)}, u32[]{:S(2)}) async-start(bf16[8,3,256,512]{3,2,1,0:T(8,128)(2,1)} %stack.2), calls=%async_computation | async-start | bytes 12582912 | tf_op jit(solution)/shard_map/all_to_all | solution.py:80
  227.2 1.6 copy.43
  228.8 1.6 copy.44
  231.2 133.2 %all-to-all-done = bf16[8,3,256,512]{3,2,1,0:T(8,128)(2,1)} async-done(((bf16[8,3,256,512]{3,2,1,0:T(8,128)(2,1)}), bf16[8,3,256,512]{3,2,1,0:T(8,128)(2,1)}, u32[]{:S(2)}, u32[]{:S(2)}) %all-to-all-start) | async-done | bytes 6291488 | tf_op jit(solution)/shard_map/all_to_all | solution.py:80
  364.4 6.1 %copy.42 = bf16[8,3,256,512]{3,2,0,1:T(8,128)(2,1)} copy(bf16[8,3,256,512]{3,2,1,0:T(8,128)(2,1)} %all-to-all-done) | data formatting | bytes 12582912 | tf_op jit(solution)/shard_map/all_to_all | solution.py:80
  (46 shorter events, 3.4 us)
Async XLA Ops:
  7.2 17.2 %copy-start.4 = (f32[16,3072]{1,0:T(8,128)S(1)}, f32[16,3072]{1,0:T(8,128)}, u32[]{:S(2)}) copy-start(f32[16,3072]{1,0:T(8,128)} %param.16) | copy-start | bytes 589828
  7.2 68.9 %all-gather.3.cloned.1.call-start = ((), (), s32[]{:S(2)}) async-start(), calls=%async_computation.1 | async-start | bytes 3538944 | tf_op jit(solution)/shard_map/all_gather | solution.py:56
  9.2 20.5 %copy-start.9 = (u32[32]{0:T(128)S(1)}, u32[32]{0:T(128)}, u32[]{:S(2)}) copy-start(u32[32]{0:T(128)} %constant.60) | copy-start | bytes 388
  9.2 43.9 %copy-start.3 = (f32[16,3072]{1,0:T(8,128)S(1)}, f32[16,3072]{1,0:T(8,128)}, u32[]{:S(2)}) copy-start(f32[16,3072]{1,0:T(8,128)} %param.15) | copy-start | bytes 589828
  9.2 189.7 %all-reduce.4.cloned.1.call-start = ((), (), s32[]{:S(2)}) async-start(), calls=%async_computation.2 | async-start | bytes 3407872 | tf_op jit(solution)/shard_map/psum | solution.py:66
  10.1 43.1 %collective-permute-start = (f32[16,1]{1,0:T(8,128)S(1)}, f32[16,1]{1,0:T(8,128)S(1)}, u32[]{:S(2)}, u32[]{:S(2)}) collective-permute-start(f32[16,1]{1,0:T(8,128)S(1)} %slice.14), channel_id=1, source_target_pairs={{0,4},{4,8},{8,12},{12,16},{16,20},{20,24},{24,28},{1,5},{5,9},{9,... | collective-permute-start | bytes 200 | tf_op jit(solution)/shard_map/ppermute | solution.py:14
  107.8 1.4 copy-start.2
  198.9 13.8 %copy-start.1 = (bf16[3,256,256]{2,1,0:T(8,128)(2,1)S(1)}, bf16[3,256,256]{2,1,0:T(8,128)(2,1)}, u32[]{:S(2)}) copy-start(bf16[3,256,256]{2,1,0:T(8,128)(2,1)} %param.18) | copy-start | bytes 1179652
  222.3 4.9 %copy-start = (f32[3,256,512]{1,2,0:T(8,128)S(1)}, f32[3,256,512]{1,2,0:T(8,128)}, u32[]{:S(2)}) copy-start(f32[3,256,512]{1,2,0:T(8,128)} %get-tuple-element.161) | copy-start | bytes 4718596
  222.3 142.1 %all-to-all-start = ((bf16[8,3,256,512]{3,2,1,0:T(8,128)(2,1)}), bf16[8,3,256,512]{3,2,1,0:T(8,128)(2,1)}, u32[]{:S(2)}, u32[]{:S(2)}) async-start(bf16[8,3,256,512]{3,2,1,0:T(8,128)(2,1)} %stack.2), calls=%async_computation | async-start | bytes 12582912 | tf_op jit(solution)/shard_map/all_to_all | solution.py:80
  228.8 1.6 copy-start.5
  228.8 1.6 copy-start.6
  228.8 1.6 copy-start.7
  228.8 1.6 copy-start.8
Sparse Core Ops, SparseCore 0:
  10.6 65.4 all-gather.2
  107.9 90.9 all-reduce.3
